TPU v7x, 32 devices: a whole 2x2x4 slice. The times are simulated.
32 devices in a mesh: kv: 8 (over z, y), tp: 4 (over x, core).
Axes of the slice: x: 2, y: 2, z: 4, core: 2. Of those that a mesh axis runs over, the one named last changes fastest.
Arguments:
- residual_in: bfloat16 [64, 2048], P(None, ('kv', 'tp')), may hold values from -14 to 14
- delta_state: float32 [64, 32, 128, 128], P('kv', 'tp'), may hold values from -1 to 1
- norm_gain_first: float32 [2048], P('kv'), may hold values from 0.1 to 1.9
- gate_first: bfloat16 [2048, 5632], P('kv', 'tp'), may hold values from -0.125 to 0.125
- up_first: bfloat16 [2048, 5632], P('kv', 'tp'), may hold values from -0.125 to 0.125
- down_first: bfloat16 [5632, 2048], P('tp', 'kv'), may hold values from -0.15625 to 0.15625
- norm_gain_mixer: float32 [2048], P('kv'), may hold values from 0.1 to 1.9
- query_weight: bfloat16 [2048, 2048], P('kv', 'tp'), may hold values from -0.125 to 0.125
- key_weight: bfloat16 [2048, 2048], P('kv', 'tp'), may hold values from -0.125 to 0.125
- value_weight: bfloat16 [2048, 4096], P('kv', 'tp'), may hold values from -0.125 to 0.125
- output_gate_weight: bfloat16 [2048, 4096], P('kv', 'tp'), may hold values from -0.125 to 0.125
- beta_weight: bfloat16 [2048, 32], P('kv'), may hold values from -0.125 to 0.125
- decay_weight: bfloat16 [2048, 32], P('kv'), may hold values from -0.125 to 0.125
- decay_rate: float32 [32], P('tp'), may hold values from -2.3 to 1.1
- decay_bias: float32 [32], P('tp'), may hold values from -1 to 1
- head_gain: float32 [128], replicated, may hold values from 0.1 to 1.9
- out_weight: bfloat16 [4096, 2048], P('tp', 'kv'), may hold values from -0.125 to 0.125
- norm_gain_second: float32 [2048], P('kv'), may hold values from 0.1 to 1.9
- gate_second: bfloat16 [2048, 5632], P('kv', 'tp'), may hold values from -0.125 to 0.125
- up_second: bfloat16 [2048, 5632], P('kv', 'tp'), may hold values from -0.125 to 0.125
- down_second: bfloat16 [5632, 2048], P('tp', 'kv'), may hold values from -0.15625 to 0.15625
Outputs:
- residual_out: bfloat16 [64, 2048], P(None, ('kv', 'tp'))
- delta_state_out: float32 [64, 32, 128, 128], P('kv', 'tp')
All inputs are finite; a program needn't handle non-finite values.
Results may differ from a plain program's by a relative error of at most 0.03.
Values may be sent and summed in bfloat16 or wider, within the bound.
A program may use at most 64 MiB of HBM per device.

v0:
```python
import jax
import jax.numpy as jnp
from jax import lax
from jax.sharding import PartitionSpec as P

D = 2048
epsilon = 1e-06


def activate(summed, square_sums, hidden_cols):
    rowscale = lax.rsqrt(square_sums / D + epsilon)[:, None]
    gate_act = summed[:, :hidden_cols] * rowscale
    up_act = summed[:, hidden_cols:] * rowscale
    return (jax.nn.silu(gate_act) * up_act).astype(jnp.bfloat16)


def feed_forward(residual, norm_gain, gate_weight, up_weight, down_weight, finish):
    as_float = residual.astype(jnp.float32)
    squares = jnp.sum(as_float * as_float, axis=1)
    scaled = (as_float * norm_gain).astype(jnp.bfloat16)
    joined = jnp.concatenate([gate_weight, up_weight], axis=1)
    partial_value = jnp.dot(scaled, joined, preferred_element_type=jnp.float32)
    hidden_cols = gate_weight.shape[1]
    summed, square_sums = (
        lax.psum(partial_value.astype(jnp.bfloat16), "kv").astype(jnp.float32),
        lax.psum(squares.astype(jnp.bfloat16), "kv").astype(jnp.float32),
    )
    hidden = activate(summed, square_sums, hidden_cols)
    projected = jnp.dot(hidden, down_weight, preferred_element_type=jnp.float32).astype(
        jnp.bfloat16
    )
    if finish:
        col_count = residual.shape[1] // lax.axis_size("tp")
        own_cols = lax.dynamic_slice_in_dim(
            as_float, lax.axis_index("tp") * col_count, col_count, 1
        )
        branch = lax.psum_scatter(projected, "tp", scatter_dimension=1, tiled=True).astype(
            jnp.float32
        )
        return (own_cols + 0.5 * branch).astype(jnp.bfloat16)
    branch = lax.psum(projected, "tp").astype(jnp.float32)
    return (as_float + 0.5 * branch).astype(jnp.bfloat16)


def unit_heads(projected, head_size):
    activated = jax.nn.silu(projected).reshape(projected.shape[0], -1, head_size)
    return activated * lax.rsqrt(jnp.sum(activated * activated, axis=-1, keepdims=True) + epsilon)


def delta_step(old_state, key_rows, queries, values, beta_gate, decay_gate):
    faded_state = old_state * decay_gate[:, :, None, None]
    predicted = jnp.einsum("rhab,rha->rhb", faded_state, key_rows, precision=lax.Precision.HIGHEST)
    correction = beta_gate[:, :, None] * (values - predicted)
    updated = faded_state + key_rows[:, :, :, None] * correction[:, :, None, :]
    reading = jnp.einsum("rhab,rha->rhb", updated, queries, precision=lax.Precision.HIGHEST)
    return (updated, reading)


def token_mixer(
    residual,
    norm_gain,
    query_weight,
    key_weight,
    value_weight,
    output_gate_weight,
    beta_weight,
    decay_weight,
    decay_rate,
    decay_bias,
    head_gain,
    out_weight,
    old_state,
):
    as_float = residual.astype(jnp.float32)
    squares = jnp.sum(as_float * as_float, axis=1)
    scaled = (as_float * norm_gain).astype(jnp.bfloat16)
    joined = jnp.concatenate([query_weight, key_weight, value_weight, output_gate_weight], axis=1)
    partial_value = jnp.dot(scaled, joined, preferred_element_type=jnp.float32)
    heads_dev = decay_rate.shape[0]
    head_start = lax.axis_index("tp") * heads_dev
    gate_cols = jnp.concatenate(
        [
            lax.dynamic_slice_in_dim(beta_weight, head_start, heads_dev, 1),
            lax.dynamic_slice_in_dim(decay_weight, head_start, heads_dev, 1),
        ],
        axis=1,
    )
    gate_part = jnp.dot(scaled, gate_cols, preferred_element_type=jnp.float32)
    row_count = old_state.shape[0]
    square_sums = lax.psum(squares, "kv")
    square_sums = lax.dynamic_slice_in_dim(
        square_sums, lax.axis_index("kv") * row_count, row_count, 0
    )
    summed, gate_summed = (
        lax.psum_scatter(
            partial_value.astype(jnp.bfloat16), "kv", scatter_dimension=0, tiled=True
        ).astype(jnp.float32),
        lax.psum_scatter(
            gate_part.astype(jnp.bfloat16), "kv", scatter_dimension=0, tiled=True
        ).astype(jnp.float32),
    )
    rowscale = lax.rsqrt(square_sums / D + epsilon)[:, None]
    summed = summed * rowscale
    gate_summed = gate_summed * rowscale
    head_size = old_state.shape[2]
    key_cols = query_weight.shape[1]
    value_cols = value_weight.shape[1]
    repeat_count = heads_dev // (key_cols // head_size)
    queries = jnp.repeat(
        unit_heads(summed[:, :key_cols], head_size) * head_size ** (-0.5), repeat_count, axis=1
    )
    key_rows = jnp.repeat(
        unit_heads(summed[:, key_cols : 2 * key_cols], head_size), repeat_count, axis=1
    )
    values = jax.nn.silu(summed[:, 2 * key_cols : 2 * key_cols + value_cols]).reshape(
        row_count, heads_dev, head_size
    )
    out_gate = jax.nn.silu(summed[:, 2 * key_cols + value_cols :]).reshape(
        row_count, heads_dev, head_size
    )
    beta_gate = jax.nn.sigmoid(gate_summed[:, :heads_dev])
    decay_gate = jnp.exp(
        -jnp.exp(decay_rate)[None, :]
        * jax.nn.softplus(gate_summed[:, heads_dev:] + decay_bias[None, :])
    )
    new_state, reading = delta_step(old_state, key_rows, queries, values, beta_gate, decay_gate)
    normed = reading * lax.rsqrt(jnp.mean(reading * reading, axis=-1, keepdims=True) + epsilon)
    normed = (
        (normed * head_gain * out_gate)
        .reshape(row_count, heads_dev * head_size)
        .astype(jnp.bfloat16)
    )
    projected = jnp.dot(
        lax.all_gather(normed, "kv", axis=0, tiled=True),
        out_weight,
        preferred_element_type=jnp.float32,
    ).astype(jnp.bfloat16)
    branch = lax.psum(projected, "tp").astype(jnp.float32)
    return ((as_float + branch).astype(jnp.bfloat16), new_state)


def body(
    residual_in,
    delta_state,
    norm_gain_first,
    gate_first,
    up_first,
    down_first,
    norm_gain_mixer,
    query_weight,
    key_weight,
    value_weight,
    output_gate_weight,
    beta_weight,
    decay_weight,
    decay_rate,
    decay_bias,
    head_gain,
    out_weight,
    norm_gain_second,
    gate_second,
    up_second,
    down_second,
):
    columns = lax.all_gather(residual_in, "tp", axis=1, tiled=True)
    after_first = feed_forward(columns, norm_gain_first, gate_first, up_first, down_first, False)
    after_mixer, new_state = token_mixer(
        after_first,
        norm_gain_mixer,
        query_weight,
        key_weight,
        value_weight,
        output_gate_weight,
        beta_weight,
        decay_weight,
        decay_rate,
        decay_bias,
        head_gain,
        out_weight,
        delta_state,
    )
    residual_out = feed_forward(
        after_mixer, norm_gain_second, gate_second, up_second, down_second, True
    )
    return (residual_out, new_state)


def solution(mesh):
    placed = (
        P(None, ("kv", "tp")),
        P("kv", "tp", None, None),
        P("kv"),
        P("kv", "tp"),
        P("kv", "tp"),
        P("tp", "kv"),
        P("kv"),
        P("kv", "tp"),
        P("kv", "tp"),
        P("kv", "tp"),
        P("kv", "tp"),
        P("kv", None),
        P("kv", None),
        P("tp"),
        P("tp"),
        P(),
        P("tp", "kv"),
        P("kv"),
        P("kv", "tp"),
        P("kv", "tp"),
        P("tp", "kv"),
    )
    return jax.shard_map(
        body,
        mesh=mesh,
        in_specs=placed,
        out_specs=(P(None, ("kv", "tp")), P("kv", "tp", None, None)),
        check_vma=False,
    )
```

profile of v0, /device:TPU:0, one launch (start us, length us, event | category | flops | bytes accessed | tf_op | source)
XLA Modules:
  0.0 322.3 jit_solution(16253293188831210375)
XLA Ops:
  7.2 0.0 copy-start
  7.2 0.0 all-reduce.4.cloned.1.call-start
  7.2 0.9 copy.27
  8.1 6.2 %all_gather.6 = bf16[64,256]{0,1:T(8,128)(2,1)S(1)} all-gather(bf16[64,64]{0,1:T(8,128)(2,1)S(1)} %copy.27), channel_id=1, replica_groups=mesh['kv'=8,'tp'=4] {'tp'}, dimensions={1}, use_global_device_ids=true | all-gather | bytes 40960 | tf_op jit(solution)/shard_map/all_gather | solution.py:165
  14.3 0.1 copy.28
  14.4 0.0 copy-start.9
  14.4 0.0 copy-start.10
  14.4 0.0 copy-start.11
  14.4 0.0 copy-start.12
  14.4 0.0 copy-start.13
  14.4 2.6 convolution_convert_fusion.2
  17.0 0.0 all-reduce.4.cloned.1.call-update
  17.0 0.0 reduce-scatter.5.cloned.1.call-start
  17.1 0.1 fusion.27
  17.2 22.4 %psum.50 = bf16[64]{0:T(256)(128)(2,1)S(1)} all-reduce(bf16[64]{0:T(256)(128)(2,1)S(1)} %fusion.27), channel_id=1, replica_groups=mesh['kv'=8,'tp'=4] {'kv'}, use_global_device_ids=true, to_apply=%region_2.0 | all-reduce | flops 64 | bytes 256 | tf_op jit(solution)/shard_map/psum | solution.py:26
  39.6 1.2 dynamic-slice
  41.5 0.7 constant_dynamic-slice_fusion
  42.2 0.7 exponential_negate_fusion
  42.9 47.6 %all-reduce.4.cloned.1.call-done = bf16[64,2816]{1,0:T(8,128)(2,1)} async-done(((bf16[64,2816]{1,0:T(8,128)(2,1)}), bf16[64,2816]{1,0:T(8,128)(2,1)}) %all-reduce.4.cloned.1.call-update) | async-done | bytes 360464 | tf_op jit(solution)/shard_map/psum | solution.py:25
  90.5 1.0 convert_element_type.96
  91.5 0.3 convolution_convert_fusion.5
  91.9 0.0 copy-start.5
  91.9 10.3 %psum.51 = bf16[64,256]{1,0:T(8,128)(2,1)S(1)} all-reduce(bf16[64,256]{1,0:T(8,128)(2,1)S(1)} %convolution_convert_fusion.5), channel_id=1, replica_groups=mesh['kv'=8,'tp'=4] {'tp'}, use_global_device_ids=true, to_apply=%region_3.4 | all-reduce | flops 16384 | bytes 65536 | tf_op jit(solution)/shard_map/psum | solution.py:41
  102.1 0.1 fusion.30
  102.3 1.1 convolution_convert_fusion.1
  103.4 0.0 reduce-scatter.5.cloned.1.call-update
  103.5 0.0 all-reduce.6.cloned.1.call-start
  103.5 19.7 %psum.52 = f32[64]{0:T(128)S(1)} all-reduce(f32[64]{0:T(128)S(1)} %get-tuple-element.4), channel_id=1, replica_groups=mesh['kv'=8,'tp'=4] {'kv'}, use_global_device_ids=true, to_apply=%region_6.7 | all-reduce | flops 64 | bytes 512 | tf_op jit(solution)/shard_map/psum | solution.py:90
  123.3 0.1 convolution_convert_fusion.6
  123.4 33.1 %all-reduce = bf16[64,16]{1,0:T(8,128)(2,1)S(1)} all-reduce(bf16[64,16]{1,0:T(8,128)(2,1)S(1)} %convolution_convert_fusion.6), channel_id=2, replica_groups=mesh['kv'=8,'tp'=4] {'kv'}, use_global_device_ids=true, to_apply=%region_4.5.clone | all-reduce | flops 1024 | bytes 4096
  156.5 0.1 add_rsqrt_fusion.4
  156.5 0.1 convert_multiply_fusion.5
  156.6 0.1 add_divide_fusion
  156.7 0.1 copy.30
  156.8 8.5 %reduce-scatter.5.cloned.1.call-done = bf16[8,3072]{1,0:T(8,128)(2,1)} async-done(((bf16[64,3072]{1,0:T(8,128)(2,1)}), bf16[8,3072]{1,0:T(8,128)(2,1)}) %reduce-scatter.5.cloned.1.call-update) | async-done | bytes 49168 | tf_op jit(solution)/shard_map/reduce_scatter | solution.py:95
  165.2 1.0 convert_multiply_fusion
  166.3 0.1 fusion.42
  166.4 0.1 fusion.43
  166.5 5.8 %fusion = f32[8,8,1,128]{3,2,1,0:T(1,128)S(1)} fusion(f32[8,8,128,1]{2,3,1,0:T(1,128)S(1)} %bitcast.57, f32[8,8,128,128]{3,2,1,0:T(8,128)} %param.22, f32[8,8]{1,0:T(8,128)S(1)} %get-tuple-element.11), kind=kOutput, calls=%fused_computation.1 | convolution fusion | flops 13631488 | bytes 4260096 | tf_op jit(solution)/shard_map/rhab,rha->rhb/dot_general | solution.py:52
  172.3 0.1 fusion.37
  172.4 1.5 multiply_add_fusion
  173.9 0.0 copy-start.4
  173.9 0.0 copy-start.3
  174.0 0.0 copy-start.14
  174.0 2.0 copy-done.2
  176.0 3.6 %fusion.59 = f32[8,8,1,128]{3,2,1,0:T(1,128)S(1)} fusion(f32[8,8,128,128]{3,2,1,0:T(8,128)S(1)} %multiply_add_fusion, f32[8,8,128,1]{2,3,1,0:T(1,128)S(1)} %bitcast.60), kind=kOutput, calls=%fused_computation.96 | convolution fusion | flops 12582912 | bytes 4259840 | tf_op jit(solution)/shard_map/rhab,rha->rhb/dot_general | solution.py:55
  179.7 0.1 fusion.35
  179.8 0.1 fusion.45
  179.9 30.6 %all_gather.7 = bf16[64,1024]{1,0:T(8,128)(2,1)S(1)} all-gather(bf16[8,1024]{1,0:T(8,128)(2,1)S(1)} %fusion.45), channel_id=1, replica_groups=mesh['kv'=8,'tp'=4] {'kv'}, dimensions={0}, use_global_device_ids=true | all-gather | bytes 147456 | tf_op jit(solution)/shard_map/all_gather | solution.py:134
  210.5 0.2 convolution_convert_fusion.4
  210.8 10.3 %psum.53 = bf16[64,256]{1,0:T(8,128)(2,1)S(1)} all-reduce(bf16[64,256]{1,0:T(8,128)(2,1)S(1)} %convolution_convert_fusion.4), channel_id=1, replica_groups=mesh['kv'=8,'tp'=4] {'tp'}, use_global_device_ids=true, to_apply=%region_11.12 | all-reduce | flops 16384 | bytes 65536 | tf_op jit(solution)/shard_map/psum | solution.py:138
  221.1 1.1 convolution_convert_fusion
  222.2 0.0 all-reduce.6.cloned.1.call-update
  222.2 0.0 reduce-scatter.7.cloned.1.call-start
  222.3 0.1 fusion.32
  222.4 19.7 %psum.55 = bf16[64]{0:T(256)(128)(2,1)S(1)} all-reduce(bf16[64]{0:T(256)(128)(2,1)S(1)} %get-tuple-element.9), channel_id=1, replica_groups=mesh['kv'=8,'tp'=4] {'kv'}, use_global_device_ids=true, to_apply=%region_14.15 | all-reduce | flops 64 | bytes 256 | tf_op jit(solution)/shard_map/psum | solution.py:26
  242.1 51.1 %all-reduce.6.cloned.1.call-done = bf16[64,2816]{1,0:T(8,128)(2,1)} async-done(((bf16[64,2816]{1,0:T(8,128)(2,1)}), bf16[64,2816]{1,0:T(8,128)(2,1)}) %all-reduce.6.cloned.1.call-update) | async-done | bytes 360464 | tf_op jit(solution)/shard_map/psum | solution.py:25
  293.2 1.0 convert_element_type.117
  294.3 0.3 convolution_convert_fusion.3
  294.6 0.7 copy.37
  295.3 0.0 reduce-scatter.7.cloned.1.call-update
  295.3 19.0 %reduce-scatter.7.cloned.1.call-done = bf16[64,64]{1,0:T(8,128)(2,1)} async-done(((bf16[256,64]{1,0:T(8,128)(2,1)}), bf16[64,64]{1,0:T(8,128)(2,1)}) %reduce-scatter.7.cloned.1.call-update) | async-done | bytes 8208
  314.3 0.8 copy.38
  315.1 0.7 add_convert_fusion
  (28 shorter events, 0.1 us)
Async XLA Ops:
  7.2 84.4 %copy-start = (bf16[1408,256]{1,0:T(8,128)(2,1)S(1)}, bf16[1408,256]{1,0:T(8,128)(2,1)}, u32[]{:S(2)}) copy-start(bf16[1408,256]{1,0:T(8,128)(2,1)} %param.26) | copy-start | bytes 2162692
  7.2 83.3 %all-reduce.4.cloned.1.call-start = ((), (), s32[]{:S(2)}) async-start(), calls=%async_computation.2 | async-start | bytes 720896 | tf_op jit(solution)/shard_map/psum | solution.py:25
  14.4 87.9 %copy-start.9 = (bf16[256,1024]{1,0:T(8,128)(2,1)S(1)}, bf16[256,1024]{1,0:T(8,128)(2,1)}, u32[]{:S(2)}) copy-start(bf16[256,1024]{1,0:T(8,128)(2,1)} %param.31) | copy-start | bytes 1572868
  14.4 87.9 %copy-start.10 = (bf16[256,1024]{1,0:T(8,128)(2,1)S(1)}, bf16[256,1024]{1,0:T(8,128)(2,1)}, u32[]{:S(2)}) copy-start(bf16[256,1024]{1,0:T(8,128)(2,1)} %param.30) | copy-start | bytes 1572868
  14.4 87.9 %copy-start.11 = (bf16[256,512]{1,0:T(8,128)(2,1)S(1)}, bf16[256,512]{1,0:T(8,128)(2,1)}, u32[]{:S(2)}) copy-start(bf16[256,512]{1,0:T(8,128)(2,1)} %param.29) | copy-start | bytes 786436
  14.4 87.9 %copy-start.12 = (bf16[256,512]{1,0:T(8,128)(2,1)S(1)}, bf16[256,512]{1,0:T(8,128)(2,1)}, u32[]{:S(2)}) copy-start(bf16[256,512]{1,0:T(8,128)(2,1)} %param.28) | copy-start | bytes 786436
  14.4 87.9 %copy-start.13 = (f32[256]{0:T(256)S(1)}, f32[256]{0:T(256)}, u32[]{:S(2)}) copy-start(f32[256]{0:T(256)} %param.27) | copy-start | bytes 3076
  17.0 148.2 %reduce-scatter.5.cloned.1.call-start = ((), (), s32[]{:S(2)}) async-start(), calls=%async_computation.3 | async-start | bytes 442368 | tf_op jit(solution)/shard_map/reduce_scatter | solution.py:95
  91.9 64.7 %copy-start.5 = (f32[8]{0:T(128)S(1)}, f32[8]{0:T(128)}, u32[]{:S(2)}) copy-start(f32[8]{0:T(128)} %param.35) | copy-start | bytes 100
  103.5 189.7 %all-reduce.6.cloned.1.call-start = ((), (), s32[]{:S(2)}) async-start(), calls=%async_computation.4 | async-start | bytes 720896 | tf_op jit(solution)/shard_map/psum | solution.py:25
  165.2 7.2 %copy-start.1 = (f32[8,8,128,128]{3,2,1,0:T(8,128)S(1)}, f32[8,8,128,128]{3,2,1,0:T(8,128)}, u32[]{:S(2)}) copy-start(f32[8,8,128,128]{3,2,1,0:T(8,128)} %param.22) | copy-start | bytes 12582916
  173.9 2.1 copy-start.2
  173.9 5.9 %copy-start.4 = (f32[128]{0:T(128)S(1)}, f32[128]{0:T(128)}, u32[]{:S(2)}) copy-start(f32[128]{0:T(128)} %param.36) | copy-start | bytes 1540
  173.9 36.6 %copy-start.3 = (bf16[1024,256]{1,0:T(8,128)(2,1)S(1)}, bf16[1024,256]{1,0:T(8,128)(2,1)}, u32[]{:S(2)}) copy-start(bf16[1024,256]{1,0:T(8,128)(2,1)} %param.37) | copy-start | bytes 1572868
  173.9 47.1 %copy-start.6 = (bf16[256,1408]{1,0:T(8,128)(2,1)S(1)}, bf16[256,1408]{1,0:T(8,128)(2,1)}, u32[]{:S(2)}) copy-start(bf16[256,1408]{1,0:T(8,128)(2,1)} %param.40) | copy-start | bytes 2162692
  174.0 47.1 %copy-start.7 = (bf16[256,1408]{1,0:T(8,128)(2,1)S(1)}, bf16[256,1408]{1,0:T(8,128)(2,1)}, u32[]{:S(2)}) copy-start(bf16[256,1408]{1,0:T(8,128)(2,1)} %param.39) | copy-start | bytes 2162692
  174.0 47.1 %copy-start.14 = (f32[256]{0:T(256)S(1)}, f32[256]{0:T(256)}, u32[]{:S(2)}) copy-start(f32[256]{0:T(256)} %param.38) | copy-start | bytes 3076
  179.7 114.5 %copy-start.8 = (bf16[1408,256]{1,0:T(8,128)(2,1)S(1)}, bf16[1408,256]{1,0:T(8,128)(2,1)}, u32[]{:S(2)}) copy-start(bf16[1408,256]{1,0:T(8,128)(2,1)} %param.41) | copy-start | bytes 2162692
  222.2 92.1 %reduce-scatter.7.cloned.1.call-start = ((), (), s32[]{:S(2)}) async-start(), calls=%async_computation.5 | async-start | bytes 81920
Sparse Core Ops, SparseCore 0:
  17.1 73.3 all-reduce.3
  103.6 61.5 reduce-scatter.4
  222.3 70.8 all-reduce.5
  295.5 18.7 reduce-scatter.6
where the time goes:
time: 323 us; the launch traced here: 322 us
  blocking collectives  152 us (47%)
  waiting for transfers between devices  126 us (39%)
  matrix products  15.2 us (5%)
  between operations  14.7 us (5%)
  other arithmetic  6.96 us (2%)
  local copies, waits for them, and re-layouts  6.68 us (2%)
    psum x2, waiting for transfers between devices, feed_forward(): lax.psum(partial_value.astype(jnp.bfloat16), 'kv').astype(jnp.float32)  98.7 us
    psum x2, blocking collectives, feed_forward(): lax.psum(squares.astype(jnp.bfloat16), 'kv').astype(jnp.float32)  42.1 us
    unnamed x1, blocking collectives  33.1 us
    all_gather x1, blocking collectives, token_mixer(): lax.all_gather(normed, 'kv', axis=0, tiled=True)  30.6 us
    psum x1, blocking collectives, token_mixer(): square_sums = lax.psum(squares, 'kv')  19.7 us
    unnamed x5, waiting for transfers between devices  19.1 us
    psum x1, blocking collectives, feed_forward(): branch = lax.psum(projected, 'tp').astype(jnp.float32)  10.3 us
    psum x1, blocking collectives, token_mixer(): branch = lax.psum(projected, 'tp').astype(jnp.float32)  10.3 us
  transfers between devices with their start and end apart: 4, of which 4 were waited for; matrix products, arithmetic and copies ran while one was open for 1% of the time, Pallas kernels for 0%

commit v1 on v0

--- a/solution.py
+++ b/solution.py
@@ -22,7 +22,9 @@
     partial_value = jnp.dot(scaled, joined, preferred_element_type=jnp.float32)
     hidden_cols = gate_weight.shape[1]
     summed, square_sums = (
-        lax.psum(partial_value.astype(jnp.bfloat16), "kv").astype(jnp.float32),
+        jnp.sum(lax.all_gather(partial_value.astype(jnp.bfloat16), "kv"), axis=0).astype(
+            jnp.float32
+        ),
         lax.psum(squares.astype(jnp.bfloat16), "kv").astype(jnp.float32),
     )
     hidden = activate(summed, square_sums, hidden_cols)

time: 323 us -> 296 us (0.916)
  waiting for transfers between devices: 126 us -> 97.2 us
    psum x2 -> x0, waiting for transfers between devices: 98.7 us -> none  [feed_forward(): lax.psum(partial_value.astype(jnp.bfloat16), 'kv').astype(jnp.float32)]
    all_gather x0 -> x2, waiting for transfers between devices: none -> 70.4 us  [feed_forward(): lax.all_gather(partial_value.astype(jnp.bfloat16), 'kv')]
    reduce_sum x0 -> x2, other arithmetic: none -> 4.59 us  [feed_forward(): jnp.sum(lax.all_gather(partial_value.astype(jnp.bfloat16), 'kv'), axis=0)]
where the time goes in v1:
time: 296 us; the launch traced here: 295 us
  blocking collectives  152 us (51%)
  waiting for transfers between devices  97.2 us (33%)
  matrix products  15.1 us (5%)
  between operations  14.7 us (5%)
  other arithmetic  9.58 us (3%)
  local copies, waits for them, and re-layouts  6.67 us (2%)
    all_gather x2, waiting for transfers between devices, feed_forward(): lax.all_gather(partial_value.astype(jnp.bfloat16), 'kv')  70.4 us
    psum x2, blocking collectives, feed_forward(): lax.psum(squares.astype(jnp.bfloat16), 'kv').astype(jnp.float32)  42.3 us
    unnamed x1, blocking collectives  33.1 us
    all_gather x1, blocking collectives, token_mixer(): lax.all_gather(normed, 'kv', axis=0, tiled=True)  30.6 us
    psum x1, blocking collectives, token_mixer(): square_sums = lax.psum(squares, 'kv')  19.1 us
    unnamed x5, waiting for transfers between devices  18.4 us
    psum x1, blocking collectives, feed_forward(): branch = lax.psum(projected, 'tp').astype(jnp.float32)  10.3 us
    psum x1, blocking collectives, token_mixer(): branch = lax.psum(projected, 'tp').astype(jnp.float32)  10.3 us
  transfers between devices with their start and end apart: 4, of which 4 were waited for; matrix products, arithmetic and copies ran while one was open for 1% of the time, Pallas kernels for 0%

profile of v1, /device:TPU:0, one launch (start us, length us, event | category | flops | bytes accessed | tf_op | source)
XLA Modules:
  0.0 295.3 jit_solution(5119203935247764952)
XLA Ops:
  7.2 0.0 copy-start
  7.2 0.0 all-gather.5.cloned.1.call-start
  7.2 0.9 copy.27
  8.1 6.2 %all_gather.18 = bf16[64,256]{0,1:T(8,128)(2,1)S(1)} all-gather(bf16[64,64]{0,1:T(8,128)(2,1)S(1)} %copy.27), channel_id=1, replica_groups=mesh['kv'=8,'tp'=4] {'tp'}, dimensions={1}, use_global_device_ids=true | all-gather | bytes 40960 | tf_op jit(solution)/shard_map/all_gather | solution.py:167
  14.3 0.1 copy.28
  14.4 2.5 convolution_convert_fusion.2
  16.8 0.0 all-gather.5.cloned.1.call-update
  16.9 0.0 reduce-scatter.5.cloned.1.call-start
  16.9 1.2 dynamic-slice
  18.8 0.1 fusion.27
  18.9 22.5 %psum.35 = bf16[64]{0:T(256)(128)(2,1)S(1)} all-reduce(bf16[64]{0:T(256)(128)(2,1)S(1)} %fusion.27), channel_id=1, replica_groups=mesh['kv'=8,'tp'=4] {'kv'}, use_global_device_ids=true, to_apply=%region_2.0 | all-reduce | flops 64 | bytes 256 | tf_op jit(solution)/shard_map/psum | solution.py:28
  41.4 0.7 constant_dynamic-slice_fusion
  42.1 0.7 exponential_negate_fusion
  42.7 33.6 %all-gather.5.cloned.1.call-done = bf16[512,2816]{1,0:T(8,128)(2,1)} async-done(((bf16[64,2816]{1,0:T(8,128)(2,1)}), bf16[512,2816]{1,0:T(8,128)(2,1)}) %all-gather.5.cloned.1.call-update) | async-done | bytes 2883600 | tf_op jit(solution)/shard_map/all_gather | solution.py:25
  76.4 2.4 reduce_sum.78
  78.8 0.0 copy-done
  78.8 0.3 convolution_convert_fusion.5
  79.1 0.0 copy-start.5
  79.2 10.3 %psum.36 = bf16[64,256]{1,0:T(8,128)(2,1)S(1)} all-reduce(bf16[64,256]{1,0:T(8,128)(2,1)S(1)} %convolution_convert_fusion.5), channel_id=1, replica_groups=mesh['kv'=8,'tp'=4] {'tp'}, use_global_device_ids=true, to_apply=%region_3.4 | all-reduce | flops 16384 | bytes 65536 | tf_op jit(solution)/shard_map/psum | solution.py:43
  89.4 0.1 fusion.30
  89.6 1.1 convolution_convert_fusion.1
  90.7 0.0 reduce-scatter.5.cloned.1.call-update
  90.8 0.0 all-gather.7.cloned.1.call-start
  90.8 19.1 %psum.37 = f32[64]{0:T(128)S(1)} all-reduce(f32[64]{0:T(128)S(1)} %get-tuple-element.4), channel_id=1, replica_groups=mesh['kv'=8,'tp'=4] {'kv'}, use_global_device_ids=true, to_apply=%region_6.7 | all-reduce | flops 64 | bytes 512 | tf_op jit(solution)/shard_map/psum | solution.py:92
  109.9 0.1 convolution_convert_fusion.6
  110.1 33.1 %all-reduce = bf16[64,16]{1,0:T(8,128)(2,1)S(1)} all-reduce(bf16[64,16]{1,0:T(8,128)(2,1)S(1)} %convolution_convert_fusion.6), channel_id=4, replica_groups=mesh['kv'=8,'tp'=4] {'kv'}, use_global_device_ids=true, to_apply=%region_4.5.clone | all-reduce | flops 1024 | bytes 4096
  143.1 0.1 add_rsqrt_fusion.4
  143.2 0.1 convert_multiply_fusion.5
  143.3 0.1 add_divide_fusion
  143.4 0.1 copy.30
  143.5 8.5 %reduce-scatter.5.cloned.1.call-done = bf16[8,3072]{1,0:T(8,128)(2,1)} async-done(((bf16[64,3072]{1,0:T(8,128)(2,1)}), bf16[8,3072]{1,0:T(8,128)(2,1)}) %reduce-scatter.5.cloned.1.call-update) | async-done | bytes 49168 | tf_op jit(solution)/shard_map/reduce_scatter | solution.py:97
  151.9 1.0 convert_multiply_fusion
  152.9 0.1 fusion.42
  153.1 0.1 fusion.43
  153.2 5.8 %fusion = f32[8,8,1,128]{3,2,1,0:T(1,128)S(1)} fusion(f32[8,8,128,1]{2,3,1,0:T(1,128)S(1)} %bitcast.61, f32[8,8,128,128]{3,2,1,0:T(8,128)} %param.22, f32[8,8]{1,0:T(8,128)S(1)} %get-tuple-element.11), kind=kOutput, calls=%fused_computation.1 | convolution fusion | flops 13631488 | bytes 4260096 | tf_op jit(solution)/shard_map/rhab,rha->rhb/dot_general | solution.py:54
  159.0 0.1 fusion.37
  159.1 1.5 multiply_add_fusion
  160.6 0.0 copy-start.2
  160.6 0.0 copy-start.4
  160.6 0.0 copy-start.3
  160.6 0.0 copy-start.6
  160.6 0.0 copy-start.7
  160.6 0.0 copy-start.14
  160.7 2.0 copy-done.2
  162.7 3.6 %fusion.59 = f32[8,8,1,128]{3,2,1,0:T(1,128)S(1)} fusion(f32[8,8,128,128]{3,2,1,0:T(8,128)S(1)} %multiply_add_fusion, f32[8,8,128,1]{2,3,1,0:T(1,128)S(1)} %bitcast.64), kind=kOutput, calls=%fused_computation.96 | convolution fusion | flops 12582912 | bytes 4259840 | tf_op jit(solution)/shard_map/rhab,rha->rhb/dot_general | solution.py:57
  166.4 0.1 fusion.35
  166.5 0.1 fusion.45
  166.6 30.6 %all_gather.21 = bf16[64,1024]{1,0:T(8,128)(2,1)S(1)} all-gather(bf16[8,1024]{1,0:T(8,128)(2,1)S(1)} %fusion.45), channel_id=1, replica_groups=mesh['kv'=8,'tp'=4] {'kv'}, dimensions={0}, use_global_device_ids=true | all-gather | bytes 147456 | tf_op jit(solution)/shard_map/all_gather | solution.py:136
  197.1 0.2 convolution_convert_fusion.4
  197.3 10.3 %psum.38 = bf16[64,256]{1,0:T(8,128)(2,1)S(1)} all-reduce(bf16[64,256]{1,0:T(8,128)(2,1)S(1)} %convolution_convert_fusion.4), channel_id=1, replica_groups=mesh['kv'=8,'tp'=4] {'tp'}, use_global_device_ids=true, to_apply=%region_11.12 | all-reduce | flops 16384 | bytes 65536 | tf_op jit(solution)/shard_map/psum | solution.py:140
  207.6 0.0 copy-start.8
  207.7 1.1 convolution_convert_fusion
  208.8 0.0 all-gather.7.cloned.1.call-update
  208.8 0.0 reduce-scatter.7.cloned.1.call-start
  208.9 0.1 fusion.32
  209.0 19.9 %psum.39 = bf16[64]{0:T(256)(128)(2,1)S(1)} all-reduce(bf16[64]{0:T(256)(128)(2,1)S(1)} %get-tuple-element.9), channel_id=1, replica_groups=mesh['kv'=8,'tp'=4] {'kv'}, use_global_device_ids=true, to_apply=%region_14.15 | all-reduce | flops 64 | bytes 256 | tf_op jit(solution)/shard_map/psum | solution.py:28
  228.9 36.7 %all-gather.7.cloned.1.call-done = bf16[512,2816]{1,0:T(8,128)(2,1)} async-done(((bf16[64,2816]{1,0:T(8,128)(2,1)}), bf16[512,2816]{1,0:T(8,128)(2,1)}) %all-gather.7.cloned.1.call-update) | async-done | bytes 2883600 | tf_op jit(solution)/shard_map/all_gather | solution.py:25
  265.6 2.2 reduce_sum.84
  267.9 0.3 convolution_convert_fusion.3
  268.2 0.7 copy.37
  268.9 0.0 reduce-scatter.7.cloned.1.call-update
  268.9 18.3 %reduce-scatter.7.cloned.1.call-done = bf16[64,64]{1,0:T(8,128)(2,1)} async-done(((bf16[256,64]{1,0:T(8,128)(2,1)}), bf16[64,64]{1,0:T(8,128)(2,1)}) %reduce-scatter.7.cloned.1.call-update) | async-done | bytes 8208
  287.3 0.8 copy.38
  288.1 0.7 add_convert_fusion
  (30 shorter events, 0.2 us)
Async XLA Ops:
  7.2 71.7 %copy-start = (bf16[1408,256]{1,0:T(8,128)(2,1)S(1)}, bf16[1408,256]{1,0:T(8,128)(2,1)}, u32[]{:S(2)}) copy-start(bf16[1408,256]{1,0:T(8,128)(2,1)} %param.26) | copy-start | bytes 2162692
  7.2 69.2 %all-gather.5.cloned.1.call-start = ((), (), s32[]{:S(2)}) async-start(), calls=%async_computation.3 | async-start | bytes 3244032 | tf_op jit(solution)/shard_map/all_gather | solution.py:25
  16.9 135.1 %reduce-scatter.5.cloned.1.call-start = ((), (), s32[]{:S(2)}) async-start(), calls=%async_computation.2 | async-start | bytes 442368 | tf_op jit(solution)/shard_map/reduce_scatter | solution.py:97
  76.4 13.2 %copy-start.9 = (bf16[256,1024]{1,0:T(8,128)(2,1)S(1)}, bf16[256,1024]{1,0:T(8,128)(2,1)}, u32[]{:S(2)}) copy-start(bf16[256,1024]{1,0:T(8,128)(2,1)} %param.31) | copy-start | bytes 1572868
  76.4 13.2 %copy-start.10 = (bf16[256,1024]{1,0:T(8,128)(2,1)S(1)}, bf16[256,1024]{1,0:T(8,128)(2,1)}, u32[]{:S(2)}) copy-start(bf16[256,1024]{1,0:T(8,128)(2,1)} %param.30) | copy-start | bytes 1572868
  76.4 13.2 %copy-start.11 = (bf16[256,512]{1,0:T(8,128)(2,1)S(1)}, bf16[256,512]{1,0:T(8,128)(2,1)}, u32[]{:S(2)}) copy-start(bf16[256,512]{1,0:T(8,128)(2,1)} %param.29) | copy-start | bytes 786436
  76.4 13.2 %copy-start.12 = (bf16[256,512]{1,0:T(8,128)(2,1)S(1)}, bf16[256,512]{1,0:T(8,128)(2,1)}, u32[]{:S(2)}) copy-start(bf16[256,512]{1,0:T(8,128)(2,1)} %param.28) | copy-start | bytes 786436
  76.4 13.2 %copy-start.13 = (f32[256]{0:T(256)S(1)}, f32[256]{0:T(256)}, u32[]{:S(2)}) copy-start(f32[256]{0:T(256)} %param.27) | copy-start | bytes 3076
  79.1 64.1 %copy-start.5 = (f32[8]{0:T(128)S(1)}, f32[8]{0:T(128)}, u32[]{:S(2)}) copy-start(f32[8]{0:T(128)} %param.35) | copy-start | bytes 100
  90.8 174.8 %all-gather.7.cloned.1.call-start = ((), (), s32[]{:S(2)}) async-start(), calls=%async_computation.4 | async-start | bytes 3244032 | tf_op jit(solution)/shard_map/all_gather | solution.py:25
  151.9 7.2 %copy-start.1 = (f32[8,8,128,128]{3,2,1,0:T(8,128)S(1)}, f32[8,8,128,128]{3,2,1,0:T(8,128)}, u32[]{:S(2)}) copy-start(f32[8,8,128,128]{3,2,1,0:T(8,128)} %param.22) | copy-start | bytes 12582916
  160.6 2.1 copy-start.2
  160.6 5.9 %copy-start.4 = (f32[128]{0:T(128)S(1)}, f32[128]{0:T(128)}, u32[]{:S(2)}) copy-start(f32[128]{0:T(128)} %param.36) | copy-start | bytes 1540
  160.6 36.5 %copy-start.3 = (bf16[1024,256]{1,0:T(8,128)(2,1)S(1)}, bf16[1024,256]{1,0:T(8,128)(2,1)}, u32[]{:S(2)}) copy-start(bf16[1024,256]{1,0:T(8,128)(2,1)} %param.37) | copy-start | bytes 1572868
  160.6 47.0 %copy-start.6 = (bf16[256,1408]{1,0:T(8,128)(2,1)S(1)}, bf16[256,1408]{1,0:T(8,128)(2,1)}, u32[]{:S(2)}) copy-start(bf16[256,1408]{1,0:T(8,128)(2,1)} %param.40) | copy-start | bytes 2162692
  160.6 47.0 %copy-start.7 = (bf16[256,1408]{1,0:T(8,128)(2,1)S(1)}, bf16[256,1408]{1,0:T(8,128)(2,1)}, u32[]{:S(2)}) copy-start(bf16[256,1408]{1,0:T(8,128)(2,1)} %param.39) | copy-start | bytes 2162692
  160.6 47.0 %copy-start.14 = (f32[256]{0:T(256)S(1)}, f32[256]{0:T(256)}, u32[]{:S(2)}) copy-start(f32[256]{0:T(256)} %param.38) | copy-start | bytes 3076
  207.6 60.2 %copy-start.8 = (bf16[1408,256]{1,0:T(8,128)(2,1)S(1)}, bf16[1408,256]{1,0:T(8,128)(2,1)}, u32[]{:S(2)}) copy-start(bf16[1408,256]{1,0:T(8,128)(2,1)} %param.41) | copy-start | bytes 2162692
  208.8 78.5 %reduce-scatter.7.cloned.1.call-start = ((), (), s32[]{:S(2)}) async-start(), calls=%async_computation.5 | async-start | bytes 81920
Sparse Core Ops, SparseCore 0:
  17.0 59.3 all-gather.4
  90.9 60.9 reduce-scatter.4
  208.9 56.5 all-gather.6
  269.1 18.1 reduce-scatter.6
